TPU v7x, 32 devices: a whole 2x2x4 slice. The times are simulated.
32 devices in a mesh: rep: 2 (over x), fs: 8 (over z, y), tp: 2 (over core).
Axes of the slice: x: 2, y: 2, z: 4, core: 2. Of those that a mesh axis runs over, the one named last changes fastest.
Arguments:
- inputs: bfloat16 [2, 3072, 2048], P('rep', 'fs', 'tp'), may hold values from -6 to 6
- gate_proj: bfloat16 [2048, 2816], P('fs', 'tp'), may hold values from -0.125 to 0.125
- value_proj: bfloat16 [2048, 2816], P('fs', 'tp'), may hold values from -0.125 to 0.125
- gate_taps: float32 [3, 2816], replicated, may hold values from -3 to 3
- value_taps: float32 [3, 2816], replicated, may hold values from -3 to 3
- out_grad: bfloat16 [2, 3072, 2816], P('rep', 'fs', 'tp'), may hold values from -6 to 6
Outputs:
- in_grad: bfloat16 [2, 3072, 2048], P('rep', 'fs', 'tp')
- gate_proj_grad: float32 [2048, 2816], P('fs', 'tp')
- value_proj_grad: float32 [2048, 2816], P('fs', 'tp')
- gate_taps_grad: float32 [3, 2816], replicated
- value_taps_grad: float32 [3, 2816], replicated
All inputs are finite; a program needn't handle non-finite values.
Results may differ from a plain program's by a relative error of at most 0.013.
Values may be sent and summed in bfloat16 or wider, within the bound.
A program may use at most 128 MiB of HBM per device.

v0:
```python
import functools

import jax
import jax.numpy as jnp
from jax import lax
from jax.experimental import pallas as pl
from jax.experimental.pallas import tpu as pltpu
from jax.sharding import PartitionSpec as P

HALO = 8


def row_length(mesh):
    axis = mesh.axis_names.index("fs")
    devices = mesh.devices.swapaxes(0, axis)
    line = devices.reshape(devices.shape[0], -1)[:, 0]
    places = [tuple(getattr(d, "coords", (i,))) for i, d in enumerate(line)]
    moved = lambda a, b: [i for i in range(len(a)) if a[i] != b[i]]
    length = 1
    while length < len(places) and moved(places[0], places[length]) == moved(places[0], places[1]):
        length += 1
    return length if len(places) % length == 0 else 1


def remote(src, dst, send, recv, **device):
    return pltpu.make_async_remote_copy(
        src_ref=src, dst_ref=dst, send_sem=send, recv_sem=recv, device_id=device, device_id_type=pl.DeviceIdType.MESH
    )


def gather_kernel(
    sizes, x_ref, g_ref, w_ref, x_all, g_all, w_all,
    w_send, w_recv, xr_send, xt_send, x_recv, xh_send, xh_recv, g_send, g_recv, gh_send, gh_recv, own_sem,
):
    reps, fs_count, tps, across = sizes
    deep = fs_count // across
    rep, fs, tp = (lax.axis_index(a) for a in ("rep", "fs", "tp"))
    z, y = fs // across, fs % across
    tokens, feats = x_ref.shape

    def other(axis_index, step, count):
        return (axis_index + step) % count

    def cols(index):
        return pl.ds(pl.multiple_of(index * feats, feats), feats)

    half_width = w_ref.shape[1] // 2

    def half(c):
        return pl.ds(c * half_width, half_width)

    def send_w(block, c, src, way, target):
        return remote(
            src.at[:, half(c)], w_all.at[block, :, half(c)], w_send.at[block, c, way], w_recv.at[block, c], fs=target
        )

    def along(block, c, src, down, up, sink):
        if down:
            @pl.when(z > 0)
            def _():
                sink(send_w(block, c, src, 0, fs - across))
        if up:
            @pl.when(z < deep - 1)
            def _():
                sink(send_w(block, c, src, 1, fs + across))

    def to_row(block, c, src, sink):
        for step in range(1, across):
            sink(send_w(block, c, src, 1 + step, z * across + other(y, step, across)))

    start = lambda c: c.start()
    sent = lambda c: c.wait_send()

    def x_main(slot, src, sem, **device):
        return remote(src, x_all.at[slot, pl.ds(0, tokens), cols(tp)], sem, x_recv.at[slot, tp], **device)

    def halos(sink):
        for side in range(2):
            near = pl.ds(0, HALO) if side == 0 else pl.ds(tokens - HALO, HALO)
            far = pl.ds(tokens + side * HALO, HALO)
            target = fs - 1 if side == 0 else fs + 1

            @pl.when((fs > 0) if side == 0 else (fs < fs_count - 1))
            def _():
                for slot in range(reps):
                    to_rep = other(rep, slot, reps)
                    for step in range(tps):
                        sink(remote(
                            x_ref.at[near], x_all.at[slot, far, cols(tp)], xh_send.at[side, slot, step],
                            xh_recv.at[side, slot, tp], rep=to_rep, fs=target, tp=other(tp, step, tps),
                        ))
                    sink(remote(
                        g_ref.at[slot, near], g_all.at[slot, far], gh_send.at[side, slot],
                        gh_recv.at[side, slot], rep=to_rep, fs=target,
                    ))

    def to_reps(sink):
        for slot in range(1, reps):
            sink(x_main(slot, x_ref, xr_send.at[slot], rep=other(rep, slot, reps)))
        for slot in range(1, reps):
            sink(remote(
                g_ref.at[slot], g_all.at[slot, pl.ds(0, tokens)], g_send.at[slot], g_recv.at[slot],
                rep=other(rep, slot, reps),
            ))

    def to_tps(slot, src, sink):
        for step in range(1, tps):
            sink(x_main(slot, src, xt_send.at[slot, step], tp=other(tp, step, tps)))

    halos(start)
    for c in range(2):
        along(fs, c, w_ref, True, True, start)
        to_row(fs, c, w_ref, start)
    to_reps(start)
    to_tps(0, x_ref, start)
    own = [
        pltpu.make_async_copy(w_ref, w_all.at[fs], own_sem.at[0]),
        pltpu.make_async_copy(x_ref, x_all.at[0, pl.ds(0, tokens), cols(tp)], own_sem.at[1]),
        pltpu.make_async_copy(g_ref.at[0], g_all.at[0, pl.ds(0, tokens)], own_sem.at[2]),
    ]
    for copy in own:
        copy.start()

    def landed(ref, sem):
        pltpu.make_async_copy(ref, ref, sem).wait()

    def hops(dist, arrive, sink):
        for sign in (-1, 1):
            block = fs + sign * dist * across

            @pl.when((z >= dist) if sign < 0 else (z + dist < deep))
            def _():
                for c in range(2):
                    if arrive:
                        landed(w_all.at[block, :, half(c)], w_recv.at[block, c])
                    along(block, c, w_all.at[block], sign > 0, sign < 0, sink)
                    if c == 0:
                        to_row(block, c, w_all.at[block], sink)
                    else:
                        level = z + sign * dist

                        @pl.when((level > 0) & (level < deep - 1))
                        def _():
                            to_row(block, c, w_all.at[block], sink)

    def across_first(dist, arrive, sink):
        for end in ((0, deep - 1) if deep > 1 else (0,)):
            @pl.when(z == end + dist if end == 0 else z == end - dist)
            def _():
                for step in range(1, across):
                    block = end * across + other(y, step, across)
                    if arrive:
                        landed(w_all.at[block, :, half(1)], w_recv.at[block, 1])
                    along(block, 1, w_all.at[block], end > 0, end == 0 and deep > 1, sink)

    def forward_x(arrive, sink):
        for slot in range(1, reps):
            mine = x_all.at[slot, pl.ds(0, tokens), cols(tp)]
            if arrive:
                landed(mine, x_recv.at[slot, tp])
            to_tps(slot, mine, sink)

    for dist in range(1, deep):
        hops(dist, True, start)
        across_first(dist - 1, True, start)
        if dist == 1:
            forward_x(True, start)
    if deep == 1:
        forward_x(True, start)
    across_first(deep - 1, True, start)

    for slot in range(reps):
        for step in range(1, tps):
            source = other(tp, step, tps)
            landed(x_all.at[slot, pl.ds(0, tokens), cols(source)], x_recv.at[slot, source])
        if slot:
            landed(g_all.at[slot, pl.ds(0, tokens)], g_recv.at[slot])
    for side in range(2):
        far = pl.ds(tokens + side * HALO, HALO)

        @pl.when((fs < fs_count - 1) if side == 0 else (fs > 0))
        def _():
            for slot in range(reps):
                for source in range(tps):
                    landed(x_all.at[slot, far, cols(source)], xh_recv.at[side, slot, source])
                landed(g_all.at[slot, far], gh_recv.at[side, slot])
    for level in range(deep):
        for step in range(1, across):
            block = level * across + other(y, step, across)
            landed(w_all.at[block, :, half(0)], w_recv.at[block, 0])
            if 0 < level < deep - 1:
                landed(w_all.at[block, :, half(1)], w_recv.at[block, 1])
    for copy in own:
        copy.wait()
    halos(sent)
    for c in range(2):
        along(fs, c, w_ref, True, True, sent)
        to_row(fs, c, w_ref, sent)
    to_reps(sent)
    to_tps(0, x_ref, sent)
    for dist in range(1, deep):
        hops(dist, False, sent)
    for dist in range(deep):
        across_first(dist, False, sent)
    forward_x(False, sent)


def gather_all(x_own, g_parts, w_own, across):
    reps, fs_count, tps = (lax.axis_size(a) for a in ("rep", "fs", "tp"))
    tokens, feats = x_own.shape
    width = g_parts.shape[2]
    ext = tokens + 2 * HALO
    sems = [
        (fs_count, 2, 1 + across), (fs_count, 2), (reps,), (reps, tps), (reps, tps), (2, reps, tps), (2, reps, tps),
        (reps,), (reps,), (2, reps), (2, reps), (3,),
    ]
    vmem, hbm = pl.BlockSpec(memory_space=pltpu.VMEM), pl.BlockSpec(memory_space=pl.ANY)
    return pl.pallas_call(
        functools.partial(gather_kernel, (reps, fs_count, tps, across)),
        out_shape=(
            jax.ShapeDtypeStruct((reps, ext, feats * tps), x_own.dtype),
            jax.ShapeDtypeStruct((reps, ext, width), g_parts.dtype),
            jax.ShapeDtypeStruct((fs_count,) + w_own.shape, w_own.dtype),
        ),
        in_specs=[vmem] * 3,
        out_specs=(hbm,) * 3,
        scratch_shapes=[pltpu.SemaphoreType.DMA(s) for s in sems],
        compiler_params=pltpu.CompilerParams(has_side_effects=True),
        name="gather_all",
    )(x_own, g_parts, w_own)


def scatter_kernel(
    sizes, grads, pv, taps, own_all, in_grad, taps_all, y_got, z_got, tp_got, rep_got, taps_got,
    y_send, y_recv, z_send, z_recv, tp_send, tp_recv, rep_send, rep_recv, own_send, own_recv,
    taps_send, taps_recv, all_send, all_recv,
):
    reps, fs_count, tps, across = sizes
    deep = fs_count // across
    rep, fs, tp = (lax.axis_index(a) for a in ("rep", "fs", "tp"))
    z, y = fs // across, fs % across
    rows, width = grads.shape[1], grads.shape[2] // 2
    tokens, feats = in_grad.shape

    def other(axis_index, step, count):
        return (axis_index + step) % count

    def part(c):
        return pl.ds(c * width, width)

    def cols(index):
        return pl.ds(pl.multiple_of(index * feats, feats), feats)

    start = lambda c: c.start()
    sent = lambda c: c.wait_send()

    def landed(ref, sem):
        pltpu.make_async_copy(ref, ref, sem).wait()

    def tap_terms(sink):
        for step in range(1, fs_count):
            sink(remote(taps, taps_got.at[step], taps_send.at[step], taps_recv.at[step], fs=other(fs, step, fs_count)))

    def y_block(c, level, sink):
        for step in range(1, across):
            to = other(y, step, across)
            sink(remote(
                grads.at[level * across + to, :, part(c)], y_got.at[step, level, c],
                y_send.at[step, level, c], y_recv.at[step, level, c], fs=z * across + to,
            ))

    def far_first(visit):
        for dist in range(deep - 1, 0, -1):
            for way in range(2):
                @pl.when((z + dist < deep) if way == 0 else (z >= dist))
                def _():
                    visit(z + dist if way == 0 else z - dist, way)

    def y_sends(sink):
        for c in range(2):
            far_first(lambda level, way: y_block(c, level, sink))
            y_block(c, z, sink)

    def to_tps(sink):
        for slot in list(range(1, reps)) + [0]:
            for step in range(1, tps):
                to = other(tp, step, tps)
                sink(remote(
                    pv.at[slot, :, cols(to)], tp_got.at[slot, step], tp_send.at[slot, step], tp_recv.at[slot, step], tp=to
                ))

    def to_reps(sink):
        for slot in range(1, reps):
            sink(remote(
                rep_got.at[0, slot], rep_got.at[1, slot], rep_send.at[slot], rep_recv.at[slot],
                rep=other(rep, reps - slot, reps),
            ))

    def z_hop(c, level, way, sink):
        sink(remote(
            grads.at[level * across + y, :, part(c)], z_got.at[way, level, c],
            z_send.at[way, level, c], z_recv.at[way, level, c], fs=fs + across if way == 0 else fs - across,
        ))

    def own_rep(c, sink):
        mine = own_all.at[rep, :, part(c)]
        for step in range(1, reps):
            sink(remote(mine, mine, own_send.at[step, c], own_recv.at[step, c], rep=other(rep, step, reps)))

    def taps_out(sink):
        mine = taps_all.at[rep, tp]
        for slot in range(reps):
            for step in range(tps):
                if slot or step:
                    sink(remote(
                        mine, mine, all_send.at[slot, step], all_recv.at[slot, step],
                        rep=other(rep, slot, reps), tp=other(tp, step, tps),
                    ))

    tap_terms(start)
    to_tps(start)
    y_sends(start)

    for way in range(2):
        @pl.when((z == 0) if way == 0 else (z == deep - 1))
        def _():
            @pl.loop(0, deep)
            def _(level):
                for c in range(2):
                    @pl.loop(0, rows // 16)
                    def _(i):
                        z_got[way, level, c, pl.ds(pl.multiple_of(i * 16, 16), 16)] = jnp.zeros((16, width), z_got.dtype)

    def own_tps(slot, at):
        total = pv[slot, at, cols(tp)].astype(jnp.float32)
        for step in range(1, tps):
            total += tp_got[slot, step, at].astype(jnp.float32)
        return total

    for slot in range(1, reps):
        for step in range(1, tps):
            landed(tp_got.at[slot, step], tp_recv.at[slot, step])

        @pl.loop(0, tokens // 16)
        def _(i):
            at = pl.ds(pl.multiple_of(i * 16, 16), 16)
            rep_got[0, slot, at] = own_tps(slot, at).astype(rep_got.dtype)
    to_reps(start)

    def add_up(c, level, ways, store):
        for step in range(1, across):
            landed(y_got.at[step, level, c], y_recv.at[step, level, c])
        for way in ways:
            @pl.when((z > 0) if way == 0 else (z < deep - 1))
            def _():
                landed(z_got.at[way, level, c], z_recv.at[way, level, c])

        @pl.loop(0, rows // 16)
        def _(i):
            at = pl.ds(pl.multiple_of(i * 16, 16), 16)
            total = grads[level * across + y, at, part(c)].astype(jnp.float32)
            for step in range(1, across):
                total += y_got[step, level, c, at].astype(jnp.float32)
            for way in ways:
                total += z_got[way, level, c, at].astype(jnp.float32)
            store(at, total.astype(grads.dtype))

    def pass_on(c, level, way):
        def store(at, value):
            grads[level * across + y, at, part(c)] = value

        add_up(c, level, (way,), store)
        z_hop(c, level, way, start)

    for c in range(2):
        far_first(lambda level, way: pass_on(c, level, way))

        def store(at, value):
            own_all[rep, at, part(c)] = value

        add_up(c, z, (0, 1), store)
        own_rep(c, start)
        if c == 0:
            total = taps[...]
            for step in range(1, fs_count):
                landed(taps_got.at[step], taps_recv.at[step])
                total += taps_got[step]
            taps_all[rep, tp] = total
            taps_out(start)
            for step in range(1, tps):
                landed(tp_got.at[0, step], tp_recv.at[0, step])
            for slot in range(1, reps):
                landed(rep_got.at[1, slot], rep_recv.at[slot])

            @pl.loop(0, tokens // 16)
            def _(i):
                at = pl.ds(pl.multiple_of(i * 16, 16), 16)
                total = own_tps(0, at)
                for slot in range(1, reps):
                    total += rep_got[1, slot, at].astype(jnp.float32)
                in_grad[at] = total.astype(in_grad.dtype)

    for slot in range(reps):
        for step in range(tps):
            if slot or step:
                landed(taps_all.at[other(rep, reps - slot, reps), other(tp, tps - step, tps)], all_recv.at[slot, step])
    for step in range(1, reps):
        for c in range(2):
            landed(own_all.at[other(rep, reps - step, reps), :, part(c)], own_recv.at[step, c])
    tap_terms(sent)
    to_tps(sent)
    y_sends(sent)
    to_reps(sent)
    for c in range(2):
        far_first(lambda level, way: z_hop(c, level, way, sent))
        own_rep(c, sent)
    taps_out(sent)


def scatter_all(grads, pv, taps, across):
    reps, fs_count, tps = (lax.axis_size(a) for a in ("rep", "fs", "tp"))
    deep = fs_count // across
    rows, width = grads.shape[1], grads.shape[2] // 2
    tokens, feats = pv.shape[1], pv.shape[2] // tps
    sem = pltpu.SemaphoreType.DMA
    pairs = [
        (across, deep, 2), (2, deep, 2), (reps, tps), (reps,), (reps, 2), (fs_count,), (reps, tps),
    ]
    vmem = pl.BlockSpec(memory_space=pltpu.VMEM)
    return pl.pallas_call(
        functools.partial(scatter_kernel, (reps, fs_count, tps, across)),
        out_shape=(
            jax.ShapeDtypeStruct((reps, rows, 2 * width), grads.dtype),
            jax.ShapeDtypeStruct((tokens, feats), pv.dtype),
            jax.ShapeDtypeStruct((reps, tps) + taps.shape, taps.dtype),
        ),
        in_specs=[vmem] * 3,
        out_specs=(vmem,) * 3,
        scratch_shapes=[
            pltpu.VMEM((across, deep, 2, rows, width), grads.dtype),
            pltpu.VMEM((2, deep, 2, rows, width), grads.dtype),
            pltpu.VMEM((reps, tps, tokens, feats), pv.dtype),
            pltpu.VMEM((2, reps, tokens, feats), pv.dtype),
            pltpu.VMEM((fs_count,) + taps.shape, taps.dtype),
        ] + [sem(p) for p in pairs for _ in range(2)],
        compiler_params=pltpu.CompilerParams(has_side_effects=True, vmem_limit_bytes=58 * 1024 * 1024),
        name="scatter_all",
    )(grads, pv, taps)


def mix_kernel(fs_count, factor, pre, g, taps, pre_cot, terms):
    reps, ext, width = g.shape
    tokens = pre_cot.shape[1]
    fs = lax.axis_index("fs")
    row = lax.broadcasted_iota(jnp.int32, (ext, 128), 0)
    has_next, has_prev = (fs < fs_count - 1).astype(jnp.int32), (fs > 0).astype(jnp.int32)
    inside = (row < tokens) | ((row < tokens + HALO) & (has_next > 0)) | ((row >= tokens + HALO) & (has_prev > 0))

    def before(x):
        return pltpu.roll(x, 1, 0)

    def after(x):
        return pltpu.roll(x, ext - 1, 0)

    terms[...] = jnp.zeros_like(terms)

    @pl.loop(0, width // 128)
    def _(j):
        spots = [pl.ds(pl.multiple_of(branch * width + j * 128, 128), 128) for branch in range(2)]
        weights = [[taps[k : k + 1, at] for k in range(3)] for at in spots]
        for slot in range(reps):
            pres = [jnp.where(inside, pre[slot, :, at].astype(jnp.float32), 0.0) for at in spots]
            around = [(before(p), p, after(p)) for p in pres]
            gate_mix, value_mix = [sum(w * p for w, p in zip(ws, ps)) for ws, ps in zip(weights, around)]
            cot_in = jnp.where(inside, g[slot, :, spots[0]].astype(jnp.float32), 0.0)
            sig = jax.nn.sigmoid(gate_mix)
            cots = (
                cot_in * value_mix * (sig * (1.0 + gate_mix * (1.0 - sig))),
                cot_in * (gate_mix * sig),
            )
            for at, ws, ps, cot in zip(spots, weights, around, cots):
                back = ws[0] * after(cot) + ws[1] * cot + ws[2] * before(cot)
                pre_cot[slot, :, at] = back[:tokens].astype(pre_cot.dtype)
                for k in range(3):
                    total = jnp.sum(ps[k][:tokens] * cot[:tokens], axis=0, keepdims=True)
                    terms[k : k + 1, at] += total * factor


def mix_all(pre, g, taps, tokens, fs_count, factor):
    reps, ext, both = pre.shape
    vmem = pl.BlockSpec(memory_space=pltpu.VMEM)
    return pl.pallas_call(
        functools.partial(mix_kernel, fs_count, factor),
        out_shape=(
            jax.ShapeDtypeStruct((reps, tokens, both), pre.dtype),
            jax.ShapeDtypeStruct((8, both), jnp.float32),
        ),
        in_specs=[vmem] * 3,
        out_specs=(vmem,) * 2,
        compiler_params=pltpu.CompilerParams(vmem_limit_bytes=40000 * 1024),
        name="mix_all",
    )(pre, g, taps)


LANES = 128
EDGE = 16


def part_width(hid, parts):
    return min(hid, -(-hid // parts // LANES) * LANES)


TUNED = (
    ("weights_y", 0), ("weights_y", 1), ("tokens_x", 0), ("own", 2), ("own", 0), ("tokens_y", 1), ("near", 0),
    ("tokens_x", 2), ("relay", 0, 1, False), ("relay", 0, 1, True), ("tokens_x", 1), ("relay", 0, 2, False),
    ("tokens_y", 0), ("near", 1), ("weights_y", 2), ("edge_out", 0), ("edge_out", 1), ("take", 1, 0, 2),
    ("take", 0, 1, 1), ("relay", 0, 2, True), ("relay", 2, 1, False), ("own", 1), ("take", 0, 1, 0),
    ("relay", 1, 1, True), ("relay", 1, 1, False), ("edge_share", 0), ("edge_share", 1), ("tokens_y", 2), ("near", 2),
    ("take", 1, 1, 1), ("last", 0), ("take", 1, 0, 0), ("relay", 1, 2, False), ("cots", 0), ("take", 1, 0, 1),
    ("tokens_core",), ("edge_pass", 0), ("edge_pass", 1), ("take", 1, 1, 2), ("take", 1, 1, 0), ("take", 0, 1, 2),
    ("take_rest",), ("project", 0), ("mix", 0), ("relay", 1, 2, True), ("relay", 2, 1, True), ("cots", 1),
    ("weight", 0), ("last", 1), ("relay", 2, 2, False), ("project", 1), ("relay", 2, 2, True), ("pass_on", 0, 2),
    ("cots", 2), ("mix", 1), ("weight", 1), ("pass_on", 0, 1), ("last", 2), ("project", 2), ("mix", 2), ("input", 0),
    ("finish", 0), ("first", 0), ("input", 2), ("pass_on", 1, 2), ("weight", 2), ("owners", 0), ("first", 2),
    ("input", 1), ("taps",), ("pass_on", 1, 1), ("first", 1), ("second", 1), ("pass_on", 2, 2), ("finish", 1),
    ("second", 0), ("pass_on", 2, 1), ("owners", 1), ("input", 3), ("finish", 2), ("taps_sum",), ("owners", 2),
)


def plan(chunks, deep):
    return TUNED if (chunks, deep) == (3, 4) else general_plan(chunks, deep)


def general_plan(chunks, deep):
    yield "weights_y", 0
    yield "tokens_y", 0
    for c in range(1, chunks):
        yield "weights_y", c
        if c < 3:
            yield "tokens_y", c
    for k in range(min(chunks, 3), 3):
        yield "tokens_y", k
    for k in (2, 0, 1):
        yield "tokens_x", k
    for side in range(2):
        yield "edge_out", side
    yield ("tokens_core",)
    for c in range(chunks):
        yield "own", c
    yield "near", 0
    yield "relay", 0, 1, False
    for side in range(2):
        yield "edge_share", side
    yield "take", 1, 0, 2
    for c in range(1, chunks):
        yield "relay", c, 1, False
    yield "take", 0, 1, 0
    yield "relay", 0, 1, True
    for c in range(1, min(chunks, 2)):
        yield "near", c
    for dist in range(2, deep):
        yield "relay", 0, dist, False
        yield "relay", 0, dist, True
    for side in range(2):
        yield "edge_pass", side
    yield "take", 0, 1, 1
    for c in range(chunks):
        yield "cots", c
    for k in (0, 1):
        yield "take", 1, 0, k
    for c in range(2, chunks):
        yield "near", c
    for c in range(1, min(chunks, 2)):
        yield "relay", c, 1, True
        for dist in range(2, deep):
            yield "relay", c, dist, False
    yield "take", 1, 1, 0
    yield "take", 0, 1, 2
    for k in (1, 2):
        yield "take", 1, 1, k
    yield ("take_rest",)
    yield "last", 0
    yield "project", 0
    for c in range(1, chunks):
        for dist in range(1, deep):
            if c > 1 and dist > 1:
                yield "relay", c, dist, False
            if c > 1 or dist > 1:
                yield "relay", c, dist, True
    for c in range(chunks):
        if c:
            yield "last", c
            yield "project", c
        yield "mix", c
        if c < max(chunks - 1, 1):
            yield "weight", c
        if c == chunks - 2:
            for early in range(chunks - 2):
                for dist in range(deep - 1, 0, -1):
                    yield "pass_on", early, dist
    yield ("taps",)
    yield "input", 0
    yield "input", 1
    yield "first", 0
    yield "input", 2
    yield "first", 1
    yield "input", 3
    yield "first", 2
    if chunks > 1:
        yield "weight", chunks - 1
    for c in range(chunks):
        if c >= chunks - 2:
            for dist in range(deep - 1, 0, -1):
                yield "pass_on", c, dist
        if c == max(chunks - 2, 0):
            for f in range(2):
                yield "second", f
            yield ("taps_sum",)
        yield "finish", c
        yield "owners", c


def fused_kernel(
    sizes, factor, x_own, gate_w, value_w, gate_taps, value_taps, g_own,
    in_grad, gate_out, value_out, gate_taps_out, value_taps_out,
    taps_mine, x_all, w_all, g_all, pre, cot, grads, from_z, fin, pv, from_tp, first_got, second_got, terms, terms_z, terms_all,
    own_sem, wy_send, wy_recv, wz_send, wz_recv, x_send, xf_send, xs_send, x_recv, hz_send, hb_send, hs_send, hx_recv,
    g_send, g_recv, hg_send, hg_recv, sz_send, sz_recv, out_send, out_recv, tp_send, tp_recv,
    s1_send, s1_recv, s2_send, s2_recv, tz_send, tz_recv, ta_send, ta_recv,
):
    deep, across, width = sizes
    rep, fs, tp = (lax.axis_index(a) for a in ("rep", "fs", "tp"))
    z, y = fs // across, fs % across
    nrep, ny, ntp = 1 - rep, 1 - y, 1 - tp
    tokens, feats = x_own.shape
    rows, hid = gate_w.shape
    main = across * tokens
    ext = main + 2 * EDGE
    chunks = width // LANES
    both = 2 * LANES
    blocks = feats // rows
    first_feats = feats * 3 // 8 // LANES * LANES
    spans = ((0, first_feats), (first_feats, feats - first_feats))
    step = tokens * 3 // 8 // 16 * 16
    pieces = ((0, step), (step, step), (2 * step, tokens - 2 * step))
    last = len(pieces) - 1
    weights = (gate_w, value_w)
    outs = (gate_out, value_out)
    others = [(dr, dy) for dr in range(2) for dy in range(2) if dr or dy]

    start = lambda c: c.start()
    sent = lambda c: c.wait_send()

    def landed(ref, sem):
        pltpu.make_async_copy(ref, ref, sem).wait()

    def moved(index, step):
        return (index + step) % 2

    def part_of(r, yy):
        return r * across + yy

    part = part_of(rep, y)

    def first_col(which):
        return jnp.minimum(which * width, hid - width)

    def live(which, c):
        return c * LANES >= which * width - first_col(which)

    def chunk_cols(which, c):
        return pl.ds(pl.multiple_of(first_col(which) + c * LANES, LANES), LANES)

    def all_cols(which):
        return pl.ds(pl.multiple_of(first_col(which), LANES), width)

    def cols(half):
        return pl.ds(pl.multiple_of(half * feats, feats), feats)

    def token_rows(yy):
        return pl.ds(pl.multiple_of(yy * tokens, 16), tokens)

    def lanes(branch):
        return pl.ds(branch * LANES, LANES)

    def near(side):
        return pl.ds(0, EDGE) if side == 0 else pl.ds(tokens - EDGE, EDGE)

    def far(side):
        return pl.ds(main + side * EDGE, EDGE)

    def gives_edge(side):
        return (y == 0) & (z > 0) if side == 0 else (y == across - 1) & (z < deep - 1)

    def has_edge(side):
        return z < deep - 1 if side == 0 else z > 0

    def takes_edge(side):
        return (y == 0) & (z < deep - 1) if side == 0 else (y == across - 1) & (z > 0)

    def greet():
        barrier = pltpu.get_barrier_semaphore()

        def hello(**device):
            pl.semaphore_signal(barrier, 1, device_id=device, device_id_type=pl.DeviceIdType.MESH)

        for dr in range(2):
            for dy in range(2):
                for dt in range(2):
                    if dr or dy or dt:
                        hello(rep=moved(rep, dr), fs=z * across + moved(y, dy), tp=moved(tp, dt))
        for step_z in range(1, deep):
            hello(fs=(z + step_z) % deep * across + y)
        for up in (True, False):
            @pl.when(z < deep - 1 if up else z > 0)
            def _():
                for dr, dy in others:
                    hello(rep=moved(rep, dr), fs=(z + 1 if up else z - 1) * across + moved(y, dy))
        next_levels = (z > 0).astype(jnp.int32) + (z < deep - 1).astype(jnp.int32)
        pl.semaphore_wait(barrier, 6 + deep + len(others) * next_levels)

    def w_across(c, sink):
        for branch, w in enumerate(weights):
            sink(remote(
                w.at[:, chunk_cols(part_of(rep, ny), c)], w_all.at[c, fs, :, lanes(branch)],
                wy_send.at[c, branch], wy_recv.at[c, branch], fs=z * across + ny,
            ))

    def w_along(c, block, up, down, sink):
        ref = w_all.at[c, block]
        if up:
            @pl.when(z < deep - 1)
            def _():
                sink(remote(ref, ref, wz_send.at[c, block, 0], wz_recv.at[c, block], fs=fs + across))
        if down:
            @pl.when(z > 0)
            def _():
                sink(remote(ref, ref, wz_send.at[c, block, 1], wz_recv.at[c, block], fs=fs - across))

    def w_local(c):
        return [
            pltpu.make_async_copy(
                w.at[:, chunk_cols(part, c)], w_all.at[c, fs, :, lanes(branch)], own_sem.at[2 * c + branch]
            ) for branch, w in enumerate(weights)
        ]

    def w_own_along(c, sink):
        w_along(c, fs, True, True, sink)

    def w_near_along(c, arrive, sink):
        block = z * across + ny
        if arrive:
            for branch in range(2):
                landed(w_all.at[c, block, :, lanes(branch)], wy_recv.at[c, branch])
        w_along(c, block, True, True, sink)

    def w_step(c, dist, near_block, forward, visit):
        for sign in (-1, 1):
            here = (z >= dist) if sign < 0 else (z + dist < deep)
            goes_on = (z < deep - 1) if sign < 0 else (z > 0)

            @pl.when(here & (goes_on if forward else jnp.logical_not(goes_on)))
            def _():
                visit((z + sign * dist) * across + (ny if near_block else y), sign)

    def w_relay(c, dist, near_block, sink=start):
        def visit(block, sign):
            if sink is start:
                landed(w_all.at[c, block], wz_recv.at[c, block])
            w_along(c, block, sign < 0, sign > 0, sink)

        w_step(c, dist, near_block, True, visit)

    def w_last(c):
        for dist in range(1, deep):
            for near_block in (False, True):
                w_step(
                    c, dist, near_block, False,
                    lambda block, sign: landed(w_all.at[c, block], wz_recv.at[c, block]),
                )

    def x_at(r, yy, k, half):
        offset, size = pieces[k]
        return x_all.at[r, pl.ds(pl.multiple_of(yy * tokens + offset, 16), size), cols(half)]

    def x_mine(k):
        return x_own.at[pl.ds(*pieces[k])]

    def x_across(k, sink):
        sink(remote(x_mine(k), x_at(rep, y, k, tp), x_send.at[1, k], x_recv.at[rep, y, k, tp], fs=z * across + ny))

    def x_over(k, sink):
        sink(remote(x_mine(k), x_at(rep, y, k, tp), x_send.at[0, k], x_recv.at[rep, y, k, tp], rep=nrep))

    def x_to_sibling(sink):
        for k in range(len(pieces)):
            sink(remote(x_mine(k), x_at(rep, y, k, tp), xs_send.at[rep, y, k], x_recv.at[rep, y, k, tp], tp=ntp))

    def x_forward(k, sink):
        if k < last:
            ref = x_at(rep, ny, k, tp)
            sink(remote(ref, ref, xf_send.at[k], x_recv.at[rep, ny, k, tp], rep=nrep))
        else:
            ref = x_at(nrep, y, k, tp)
            sink(remote(ref, ref, xf_send.at[k], x_recv.at[nrep, y, k, tp], fs=z * across + ny))

    def x_take(r, yy, k, forward):
        x_landed(r, yy, k, tp)
        if forward:
            x_forward(k, start)
        x_share(r, yy, k, start)

    def x_share(r, yy, k, sink):
        ref = x_at(r, yy, k, tp)
        sink(remote(ref, ref, xs_send.at[r, yy, k], x_recv.at[r, yy, k, tp], tp=ntp))

    def x_landed(r, yy, k, half):
        landed(x_at(r, yy, k, half), x_recv.at[r, yy, k, half])

    def edge_out(side, sink):
        target = fs - across if side == 0 else fs + across

        @pl.when(gives_edge(side))
        def _():
            sink(remote(
                x_own.at[near(side)], x_all.at[rep, far(side), cols(tp)], hz_send.at[side],
                hx_recv.at[side, rep, tp], fs=target,
            ))
            level = z - 1 if side == 0 else z + 1
            for dr in range(2):
                for dy in range(2):
                    r, yy = moved(rep, dr), moved(y, dy)
                    sink(remote(
                        g_own.at[near(side), all_cols(part_of(r, yy))], g_all.at[rep, far(side)],
                        hg_send.at[side, dr, dy], hg_recv.at[side, rep], rep=r, fs=level * across + yy,
                    ))

    def edge_at(side, r, half):
        return x_all.at[r, far(side), cols(half)]

    def edge_share(side, sink=start):
        @pl.when(takes_edge(side))
        def _():
            ref = edge_at(side, rep, tp)
            if sink is start:
                landed(ref, hx_recv.at[side, rep, tp])
            for dr, dy in others:
                sink(remote(
                    ref, ref, hb_send.at[side, dr, dy], hx_recv.at[side, rep, tp],
                    rep=moved(rep, dr), fs=z * across + moved(y, dy),
                ))
            sink(remote(ref, ref, hs_send.at[side, rep], hx_recv.at[side, rep, tp], tp=ntp))

    def edge_pass(side, sink=start):
        for r in (rep, nrep):
            @pl.when(has_edge(side) & jnp.logical_not(takes_edge(side) & (r == rep)))
            def _():
                ref = edge_at(side, r, tp)
                if sink is start:
                    landed(ref, hx_recv.at[side, r, tp])
                sink(remote(ref, ref, hs_send.at[side, r], hx_recv.at[side, r, tp], tp=ntp))

    def edge_landed(side):
        @pl.when(has_edge(side))
        def _():
            for r in range(2):
                landed(edge_at(side, r, ntp), hx_recv.at[side, r, ntp])
                landed(g_all.at[r, far(side)], hg_recv.at[side, r])

    def g_direct(c, sink):
        for dr, dy in others:
            r, yy = moved(rep, dr), moved(y, dy)
            sink(remote(
                g_own.at[:, chunk_cols(part_of(r, yy), c)], g_all.at[rep, token_rows(y), pl.ds(c * LANES, LANES)],
                g_send.at[c, dr, dy], g_recv.at[c, rep, y], rep=r, fs=z * across + yy,
            ))

    def g_landed(c):
        for dr, dy in others:
            r, yy = moved(rep, dr), moved(y, dy)
            landed(g_all.at[r, token_rows(yy), pl.ds(c * LANES, LANES)], g_recv.at[c, r, yy])

    x_local = pltpu.make_async_copy(
        x_own, x_all.at[rep, token_rows(y), cols(tp)], own_sem.at[2 * chunks]
    )
    g_local = pltpu.make_async_copy(
        g_own.at[:, all_cols(part)], g_all.at[rep, token_rows(y)], own_sem.at[2 * chunks + 1]
    )

    tap_cols = pl.ds(pl.multiple_of(tp * hid + first_col(part), LANES), width)
    taps_local = [
        pltpu.make_async_copy(ref.at[:, tap_cols], taps_mine.at[b], own_sem.at[2 * chunks + 2 + b])
        for b, ref in enumerate((gate_taps, value_taps))
    ]

    def chunk_lanes(c):
        return pl.ds(c * both, both)

    def project(c):
        @pl.loop(0, 2)
        def _(slot):
            total = jnp.dot(
                x_all[slot], w_all[c].reshape(-1, both), preferred_element_type=jnp.float32
            )
            pre[slot] = total.astype(pre.dtype)

    def mix(c):
        row = lax.broadcasted_iota(jnp.int32, (ext, LANES), 0)
        has_next, has_prev = (z < deep - 1).astype(jnp.int32), (z > 0).astype(jnp.int32)
        inside = (row < main) | ((row < main + EDGE) & (has_next > 0)) | ((row >= main + EDGE) & (has_prev > 0))
        counted = inside & (live(part, c).astype(jnp.int32) > 0)
        taps = [[taps_mine[b, k : k + 1, pl.ds(c * LANES, LANES)] for k in range(3)] for b in range(2)]
        terms[:, pl.ds(c * LANES, LANES)] = jnp.zeros((8, LANES), jnp.float32)

        def before(v):
            return pltpu.roll(v, 1, 0)

        def after(v):
            return pltpu.roll(v, ext - 1, 0)

        @pl.loop(0, 2)
        def _(slot):
            pres = [jnp.where(inside, pre[slot, :, lanes(b)].astype(jnp.float32), 0.0) for b in range(2)]
            around = [(before(p), p, after(p)) for p in pres]
            gate_mix, value_mix = [sum(w * p for w, p in zip(ws, ps)) for ws, ps in zip(taps, around)]
            cot_in = jnp.where(counted, g_all[slot, :, pl.ds(c * LANES, LANES)].astype(jnp.float32), 0.0)
            sig = jax.nn.sigmoid(gate_mix)
            cots = (
                cot_in * value_mix * (sig * (1.0 + gate_mix * (1.0 - sig))),
                cot_in * (gate_mix * sig),
            )
            for b in range(2):
                ws, ps, one = taps[b], around[b], cots[b]
                back = ws[0] * after(one) + ws[1] * one + ws[2] * before(one)
                cot[slot, :, pl.ds(c * both + b * LANES, LANES)] = back[:main].astype(cot.dtype)
                for k in range(3):
                    total = jnp.sum(ps[k][:main] * one[:main], axis=0, keepdims=True)
                    terms[2 * k + b : 2 * k + b + 1, pl.ds(c * LANES, LANES)] += total * factor

    def far_first(visit):
        @pl.loop(0, 2 * deep - 1)
        def _(i):
            dist = deep - 1 - i // 2
            level = jnp.where(i % 2 == 0, z + dist, z - dist)

            @pl.when((level >= 0) & (level < deep))
            def _():
                visit(level)

    def sum_hop(c, block, up, sink):
        way = 0 if up else 1
        sink(remote(
            grads.at[c, block], from_z.at[way, c, block], sz_send.at[c, block], sz_recv.at[way, c, block],
            fs=fs + across if up else fs - across,
        ))

    def weight_terms(c):
        def visit(level):
            for yy in range(across):
                block = level * across + yy
                at = pl.ds(pl.multiple_of(block * rows, rows), rows)
                total = sum(
                    lax.dot_general(
                        x_all[slot, :main, at], cot[slot, :, chunk_lanes(c)], (((0,), (0,)), ((), ())),
                        preferred_element_type=jnp.float32,
                    ) for slot in range(2)
                )
                grads[c, block] = (total * factor).astype(grads.dtype)
            for up in (True, False):
                @pl.when((level > z) & (z == 0) if up else (level < z) & (z == deep - 1))
                def _():
                    for yy in range(across):
                        sum_hop(c, level * across + yy, up, start)

        far_first(visit)

    def pass_on(c, dist):
        for up in (True, False):
            level = z + dist if up else z - dist

            @pl.when((z > 0) & (z < deep - 1) & ((level < deep) if up else (level >= 0)))
            def _():
                way = 0 if up else 1
                for yy in range(across):
                    block = level * across + yy
                    landed(from_z.at[way, c, block], sz_recv.at[way, c, block])
                    total = grads[c, block].astype(jnp.float32) + from_z[way, c, block].astype(jnp.float32)
                    grads[c, block] = total.astype(grads.dtype)
                    sum_hop(c, block, up, start)

    def sums_sent(c):
        def visit(level):
            for up in (True, False):
                @pl.when((level > z) if up else (level < z))
                def _():
                    for yy in range(across):
                        sum_hop(c, level * across + yy, up, sent)

        far_first(visit)

    def to_owners(c, same, sink):
        here = chunk_cols(part, c)
        for branch, out in enumerate(outs):
            sems = out_send.at[c, branch, 0 if same else 1], out_recv.at[c, branch, rep, y]
            if same:
                sink(remote(out.at[:, here], out.at[:, here], *sems, rep=nrep))
            else:
                sink(remote(fin.at[c, :, lanes(branch)], out.at[:, here], *sems, fs=z * across + ny))

    def owners_pass(c, sink=start):
        source = part_of(rep, ny)

        @pl.when(live(source, c))
        def _():
            for branch, out in enumerate(outs):
                ref, sem = out.at[:, chunk_cols(source, c)], out_recv.at[c, branch, rep, ny]
                if sink is start:
                    landed(ref, sem)
                sink(remote(ref, ref, out_send.at[c, branch, 2], sem, rep=nrep))

    def owners_last(c):
        for yy in (y, ny):
            source = part_of(nrep, yy)

            @pl.when(live(source, c))
            def _():
                for branch, out in enumerate(outs):
                    landed(out.at[:, chunk_cols(source, c)], out_recv.at[c, branch, nrep, yy])

    def finish(c):
        for same in (False, True):
            block = z * across + (y if same else ny)
            for way in range(2):
                @pl.when(z > 0 if way == 0 else z < deep - 1)
                def _():
                    landed(from_z.at[way, c, block], sz_recv.at[way, c, block])
            total = grads[c, block].astype(jnp.float32)
            for way in range(2):
                total += from_z[way, c, block].astype(jnp.float32)
            total = total.astype(grads.dtype)

            @pl.when(live(part, c))
            def _():
                if same:
                    for branch, out in enumerate(outs):
                        out[:, chunk_cols(part, c)] = total[:, branch * LANES : (branch + 1) * LANES]
                else:
                    fin[c] = total
                to_owners(c, same, start)

    def input_terms(dr, dy):
        r, yy = moved(rep, dr), moved(y, dy)
        q = part_of(r, yy)

        @pl.loop(0, 2 * blocks)
        def _(i):
            half = jnp.where(i < blocks, ntp, tp)
            j = i % blocks
            total = sum(
                lax.dot_general(
                    cot[r, token_rows(yy), chunk_lanes(c)], w_all[c, half * blocks + j],
                    (((1,), (1,)), ((), ())), preferred_element_type=jnp.float32,
                ) for c in range(chunks)
            )
            pv[half, q, :, pl.ds(pl.multiple_of(j * rows, rows), rows)] = total.astype(pv.dtype)

        tp_hop(q, start)

    def tp_hop(q, sink):
        sink(remote(pv.at[ntp, q], from_tp.at[q], tp_send.at[q], tp_recv.at[q], tp=ntp))

    def f_cols(f):
        return pl.ds(*spans[f])

    def first_hop(f, k, sink):
        q = part_of(nrep, ny) if k else part_of(nrep, y) if f == 0 else part_of(rep, ny)
        target = dict(rep=nrep) if f == 0 else dict(fs=z * across + ny)
        sink(remote(pv.at[tp, q, :, f_cols(f)], first_got.at[f, k, :, pl.ds(0, spans[f][1])], s1_send.at[f, k], s1_recv.at[f, k], **target))

    def second_hop(f, sink):
        q = part_of(rep, ny) if f == 0 else part_of(nrep, y)
        target = dict(fs=z * across + ny) if f == 0 else dict(rep=nrep)
        sink(remote(pv.at[tp, q, :, f_cols(f)], second_got.at[f, :, pl.ds(0, spans[f][1])], s2_send.at[f], s2_recv.at[f], **target))

    def row_tiles(body):
        @pl.loop(0, tokens // 16)
        def _(i):
            body(pl.ds(pl.multiple_of(i * 16, 16), 16))

    def add_sibling(q):
        landed(from_tp.at[q], tp_recv.at[q])

        def body(at):
            total = pv[tp, q, at].astype(jnp.float32) + from_tp[q, at].astype(jnp.float32)
            pv[tp, q, at] = total.astype(pv.dtype)

        row_tiles(body)

    def input_first(dr, dy):
        add_sibling(part_of(moved(rep, dr), moved(y, dy)))
        if dr:
            first_hop(0, dy, start)
        if dy:
            first_hop(1, dr, start)

    def input_second(f):
        q = part_of(rep, ny) if f == 0 else part_of(nrep, y)
        landed(first_got.at[f, 1, :, pl.ds(0, spans[f][1])], s1_recv.at[f, 1])

        def body(at):
            total = pv[tp, q, at, f_cols(f)].astype(jnp.float32)
            total += first_got[f, 1, at, : spans[f][1]].astype(jnp.float32)
            pv[tp, q, at, f_cols(f)] = total.astype(pv.dtype)

        row_tiles(body)
        second_hop(f, start)

    def input_last():
        landed(from_tp.at[part], tp_recv.at[part])
        for f in range(2):
            landed(first_got.at[f, 0, :, pl.ds(0, spans[f][1])], s1_recv.at[f, 0])
            landed(second_got.at[f, :, pl.ds(0, spans[f][1])], s2_recv.at[f])

        def body(at):
            for f in range(2):
                total = pv[tp, part, at, f_cols(f)].astype(jnp.float32) + from_tp[part, at, f_cols(f)].astype(jnp.float32)
                total += first_got[f, 0, at, : spans[f][1]].astype(jnp.float32) + second_got[f, at, : spans[f][1]].astype(jnp.float32)
                in_grad[at, f_cols(f)] = total.astype(in_grad.dtype)

        row_tiles(body)

    def taps_along(sink):
        for step in range(1, deep):
            to = (z + step) % deep
            sink(remote(
                terms_z.at[z], terms_z.at[z], tz_send.at[step], tz_recv.at[z], fs=to * across + y
            ))

    def taps_start():
        terms_z[z] = terms[...]
        taps_along(start)

    def taps_out(sink):
        ref = terms_all.at[rep, y, tp]
        for dr in range(2):
            for dy in range(2):
                for dt in range(2):
                    if dr or dy or dt:
                        sink(remote(
                            ref, ref, ta_send.at[dr, dy, dt], ta_recv.at[rep, y, tp],
                            rep=moved(rep, dr), fs=z * across + moved(y, dy), tp=moved(tp, dt),
                        ))

    def taps_sum():
        for step in range(1, deep):
            source = (z + step) % deep
            landed(terms_z.at[source], tz_recv.at[source])
        terms_all[rep, y, tp] = sum(terms_z[level] for level in range(deep))
        taps_out(start)

    def taps_last():
        for dr in range(2):
            for dy in range(2):
                for dt in range(2):
                    if dr or dy or dt:
                        at = (moved(rep, dr), moved(y, dy), moved(tp, dt))
                        landed(terms_all.at[at], ta_recv.at[at])
        for r in range(2):
            for yy in range(across):
                which = r * across + yy
                first = min(which * width, hid - width)
                skip = which * width - first
                for half in range(2):
                    for branch, out in enumerate((gate_taps_out, value_taps_out)):
                        for k in range(3):
                            if skip < width:
                                begin = half * hid + first + skip
                                out[k : k + 1, begin : begin + width - skip] = terms_all[
                                    r, yy, half, 2 * k + branch : 2 * k + branch + 1, skip:
                                ]

    for c in range(chunks):
        for copy in w_local(c):
            copy.start()
    x_local.start()
    g_local.start()
    for copy in taps_local:
        copy.start()
    for way in range(2):
        @pl.when((z == 0) if way == 0 else (z == deep - 1))
        def _():
            for c in range(chunks):
                for yy in range(across):
                    from_z[way, c, z * across + yy] = jnp.zeros((rows, both), from_z.dtype)
    greet()

    def w_own(c):
        for copy in w_local(c):
            copy.wait()
        w_own_along(c, start)

    def take(dr, dy, k):
        x_take(moved(rep, dr), moved(y, dy), k, (not dr) if k < last else (not dy))

    def take_rest():
        x_local.wait()
        g_local.wait()
        for copy in taps_local:
            copy.wait()
        for r in range(2):
            for yy in range(across):
                for k in range(len(pieces)):
                    x_landed(r, yy, k, ntp)
        for side in range(2):
            edge_landed(side)

    def mix_chunk(c):
        g_landed(c)
        mix(c)

    offsets = ((1, 1), (0, 1), (1, 0), (0, 0))
    actions = dict(
        weights_y=lambda c: w_across(c, start),
        tokens_y=lambda k: x_across(k, start),
        tokens_x=lambda k: x_over(k, start),
        tokens_core=lambda: x_to_sibling(start),
        edge_out=lambda side: edge_out(side, start),
        own=w_own,
        near=lambda c: w_near_along(c, True, start),
        relay=w_relay,
        edge_share=edge_share,
        edge_pass=edge_pass,
        take=take,
        cots=lambda c: g_direct(c, start),
        take_rest=take_rest,
        last=w_last,
        project=project,
        mix=mix_chunk,
        weight=weight_terms,
        pass_on=pass_on,
        finish=finish,
        owners=owners_pass,
        taps=taps_start,
        taps_sum=taps_sum,
        input=lambda i: input_terms(*offsets[i]),
        first=lambda i: input_first(*offsets[i]),
        second=input_second,
    )
    for name, *args in plan(chunks, deep):
        actions[name](*args)
    input_last()
    taps_last()
    for c in range(chunks):
        owners_last(c)
    for side in range(2):
        edge_out(side, sent)
        edge_share(side, sent)
        edge_pass(side, sent)
    x_to_sibling(sent)
    for k in range(len(pieces)):
        x_across(k, sent)
        x_over(k, sent)
        x_forward(k, sent)
        for dr, dy in others:
            x_share(moved(rep, dr), moved(y, dy), k, sent)
    for c in range(chunks):
        w_across(c, sent)
        w_own_along(c, sent)
        w_near_along(c, False, sent)
        for dist in range(1, deep):
            for near_block in (False, True):
                w_relay(c, dist, near_block, sent)
        g_direct(c, sent)
        sums_sent(c)

        @pl.when(live(part, c))
        def _():
            for same in (False, True):
                to_owners(c, same, sent)

        owners_pass(c, sent)
    for dr in range(2):
        for dy in range(2):
            tp_hop(part_of(moved(rep, dr), moved(y, dy)), sent)
    for f in range(2):
        for k in range(2):
            first_hop(f, k, sent)
        second_hop(f, sent)
    taps_along(sent)
    taps_out(sent)


def fused_all(across, x_own, gate_w, value_w, gate_taps, value_taps, g_own):
    reps, fs_count, tps = (lax.axis_size(a) for a in ("rep", "fs", "tp"))
    deep = fs_count // across
    tokens, feats = x_own.shape
    rows, hid = gate_w.shape
    width = part_width(hid, reps * across)
    chunks = width // LANES
    both = 2 * LANES
    main = across * tokens
    ext = main + 2 * EDGE
    parts = reps * across
    factor = float(tokens * fs_count * reps) ** (-0.5)
    dtype = x_own.dtype
    f32 = jnp.float32
    sem = pltpu.SemaphoreType.DMA
    sems = [
        (2 * chunks + 4,), (chunks, 2), (chunks, 2), (chunks, fs_count, 2), (chunks, fs_count), (2, 3), (3,),
        (reps, across, 3), (reps, across, 3, tps), (2,), (2, 2, 2), (2, reps), (2, reps, tps),
        (chunks, 2, 2), (chunks, reps, across), (2, 2, 2), (2, reps), (chunks, fs_count), (2, chunks, fs_count),
        (chunks, 2, 3), (chunks, 2, reps, across), (parts,), (parts,),
        (2, 2), (2, 2), (2,), (2,), (deep,), (deep,), (2, 2, 2), (reps, across, tps),
    ]
    buffers = [
        ((2, 3, width), f32), ((reps, ext, tps * feats), dtype), ((chunks, fs_count, rows, both), dtype), ((reps, ext, width), dtype),
        ((reps, ext, both), dtype), ((reps, main, 2 * width), dtype), ((chunks, fs_count, rows, both), dtype),
        ((2, chunks, fs_count, rows, both), dtype), ((chunks, rows, both), dtype),
        ((tps, parts, tokens, feats), dtype), ((parts, tokens, feats), dtype),
        ((2, 2, tokens, feats), dtype), ((2, tokens, feats), dtype),
        ((8, width), f32), ((deep, 8, width), f32), ((reps, across, tps, 8, width), f32),
    ]
    vmem, hbm = pl.BlockSpec(memory_space=pltpu.VMEM), pl.BlockSpec(memory_space=pl.ANY)
    return pl.pallas_call(
        functools.partial(fused_kernel, (deep, across, width), factor),
        out_shape=(
            jax.ShapeDtypeStruct((tokens, feats), dtype),
            jax.ShapeDtypeStruct((rows, hid), dtype),
            jax.ShapeDtypeStruct((rows, hid), dtype),
            jax.ShapeDtypeStruct(gate_taps.shape, f32),
            jax.ShapeDtypeStruct(value_taps.shape, f32),
        ),
        in_specs=[hbm] * 6,
        out_specs=(vmem,) * 5,
        scratch_shapes=[pltpu.VMEM(*b) for b in buffers] + [sem(s) for s in sems],
        compiler_params=pltpu.CompilerParams(has_side_effects=True, collective_id=0, vmem_limit_bytes=60 * 1024 * 1024),
        name="fused_all",
    )(x_own, gate_w, value_w, gate_taps, value_taps, g_own)


def store_kernel(in_grad, gate, value, gate_taps, value_taps, *refs):
    outs, held, (gate_wide, value_wide, load_sem, sem) = refs[:5], refs[5:10], refs[10:]
    loads = [
        pltpu.make_async_copy(src, dst, load_sem.at[k])
        for k, (src, dst) in enumerate(zip((in_grad, gate, value, gate_taps, value_taps), held))
    ]
    order = (1, 2, 0, 3, 4)
    for k in order:
        loads[k].start()
    copies = []
    for k in order:
        loads[k].wait()
        src = held[k]
        if k in (1, 2):
            src = gate_wide if k == 1 else value_wide
            src[...] = held[k][...].astype(src.dtype)
        copies.append(pltpu.make_async_copy(src, outs[k], sem.at[k]))
        copies[-1].start()
    for copy in copies:
        copy.wait()


def store_all(*arrays):
    hbm = pl.BlockSpec(memory_space=pl.ANY)
    wide = jax.ShapeDtypeStruct(arrays[1].shape, jnp.float32)
    outs = [jax.ShapeDtypeStruct(a.shape, a.dtype) for a in arrays]
    outs[1:3] = wide, wide
    sem = pltpu.SemaphoreType.DMA((5,))
    return pl.pallas_call(
        store_kernel,
        out_shape=tuple(outs),
        in_specs=[hbm] * 5,
        out_specs=(hbm,) * 5,
        scratch_shapes=[pltpu.VMEM(a.shape, a.dtype) for a in arrays] + [pltpu.VMEM(wide.shape, wide.dtype)] * 2 + [sem] * 2,
        compiler_params=pltpu.CompilerParams(vmem_limit_bytes=60 * 1024 * 1024),
        name="store_all",
    )(*arrays)


def fits_plane(across, inputs, gate_proj):
    reps, fs_count, tps = (lax.axis_size(a) for a in ("rep", "fs", "tp"))
    tokens, feats = inputs.shape[1:]
    rows, hid = gate_proj.shape
    parts = reps * across
    width = part_width(hid, parts)
    return (
        reps == across == tps == 2 and fs_count > across and tokens % 16 == 0 and tokens >= 48
        and hid % LANES == 0 and rows % LANES == 0 and feats % rows == 0 and feats % (2 * LANES) == 0
        and 4 * parts * width <= 5 * hid
    )


def shards(across, inputs, gate_proj, value_proj, gate_taps, value_taps, out_grad):
    if fits_plane(across, inputs, gate_proj):
        in_grad, gate_grad, value_grad, gate_terms, value_terms = store_all(
            *fused_all(across, inputs[0], gate_proj, value_proj, gate_taps, value_taps, out_grad[0])
        )
        return in_grad[None], gate_grad, value_grad, gate_terms, value_terms

    contract_cols = (((1,), (1,)), ((), ()))
    contract_rows = (((0,), (0,)), ((), ()))
    reps, fs_count = lax.axis_size("rep"), lax.axis_size("fs")
    rep = lax.axis_index("rep")
    tokens, feats = inputs.shape[1:]
    hid = gate_proj.shape[1]
    width = min(hid, -(-hid // reps // 128) * 128)
    last = hid - width

    def start_of(part):
        return jnp.minimum(part * width, last)

    first = start_of(rep)
    dead = rep * width - first
    live = jnp.arange(width) >= dead

    def part_cols(x, part):
        return lax.dynamic_slice_in_dim(x, start_of(part), width, x.ndim - 1)

    w_own = jnp.concatenate(
        [jnp.where(live, part_cols(w, rep), jnp.zeros((), w.dtype)) for w in (gate_proj, value_proj)], axis=1
    )
    g_parts = jnp.stack([part_cols(out_grad[0], (rep + step) % reps) for step in range(reps)])
    x_all, g_all, w_all = gather_all(inputs[0], g_parts, w_own, across)
    w_all = w_all.reshape(-1, 2 * width)

    ext = tokens + 2 * HALO
    pre = jnp.dot(x_all.reshape(reps * ext, -1), w_all, preferred_element_type=jnp.float32)
    pre = pre.astype(jnp.bfloat16).reshape(reps, ext, 2 * width)
    tap_start = lax.axis_index("tp") * hid + first
    taps = jnp.concatenate(
        [lax.dynamic_slice_in_dim(t, tap_start, width, 1) for t in (gate_taps, value_taps)], axis=1
    )
    factor = float(tokens * fs_count * reps) ** (-0.5)
    pre_cot, tap_terms = mix_all(pre, g_all, taps, tokens, fs_count, factor)
    pre_cot = pre_cot.reshape(reps * tokens, 2 * width)
    tap_terms = tap_terms[:3]

    grads = lax.dot_general(
        x_all[:, :tokens].reshape(reps * tokens, -1), pre_cot, contract_rows, preferred_element_type=jnp.float32
    )
    grads = (grads * factor).astype(jnp.bfloat16).reshape(fs_count, -1, 2 * width)
    partial_value = lax.dot_general(pre_cot, w_all, contract_cols, preferred_element_type=jnp.float32)
    partial_value = partial_value.astype(jnp.bfloat16).reshape(reps, tokens, -1)
    lanes = -(-tap_terms.size // 1024) * 128
    tap_terms = jnp.pad(tap_terms.reshape(-1), (0, 8 * lanes - tap_terms.size)).reshape(8, lanes)
    own, in_grad, tap_all = scatter_all(grads, partial_value, tap_terms, across)

    skips = [max(0, p * width - last) for p in range(reps)]
    proj_grads = [
        jnp.concatenate(
            [own[p, :, branch * width + skips[p] : (branch + 1) * width] for p in range(reps)], axis=1
        ).astype(jnp.float32)
        for branch in range(2)
    ]
    tap_all = tap_all.reshape(reps, -1, 8 * lanes)[:, :, : 6 * width].reshape(reps, -1, 3, 2, width)
    taps_out = jnp.concatenate(
        [tap_all[p, half, :, :, skips[p] :] for half in range(tap_all.shape[1]) for p in range(reps)], axis=2
    )
    return in_grad[None], proj_grads[0], proj_grads[1], taps_out[:, 0], taps_out[:, 1]


def solution(mesh):
    placed = (P("rep", "fs", "tp"), P("fs", "tp"), P("fs", "tp"), P(), P(), P("rep", "fs", "tp"))
    return jax.shard_map(
        functools.partial(shards, row_length(mesh)),
        mesh=mesh,
        in_specs=placed,
        out_specs=(P("rep", "fs", "tp"), P("fs", "tp"), P("fs", "tp"), P(), P()),
        check_vma=False,
    )
```

profile of v0, /device:TPU:0, one launch (start us, length us, event | category | flops | bytes accessed | tf_op | source)
XLA Modules:
  0.0 116.5 jit_solution(17553988452208591277)
XLA Ops:
  0.6 112.7 %fused_all.1 = (bf16[384,1024]{1,0:T(8,128)(2,1)}, bf16[256,1408]{1,0:T(8,128)(2,1)}, bf16[256,1408]{1,0:T(8,128)(2,1)}, f32[3,2816]{1,0:T(4,128)}, f32[3,2816]{1,0:T(4,128)}) custom-call(bf16[384,1024]{1,0:T(8,128)(2,1)} %bitcast.4, bf16[256,1408]{1,0:T(8,128)(2,1)} %gate_w.1, bf16[256,1408]{1,0:T(8,128)(2,1)} %value_w.1, f32[3,2816]{1,0:T(4,128)} %gate_taps.1, ...), custom_call_target="tpu_custom_call" | custom-call | tf_op jit(solution)/shard_map/fused_all/pallas_call | solution.py:1324
  113.3 3.1 %store_all.1 = (bf16[384,1024]{1,0:T(8,128)(2,1)}, f32[256,1408]{1,0:T(8,128)}, f32[256,1408]{1,0:T(8,128)}, f32[3,2816]{1,0:T(4,128)}, f32[3,2816]{1,0:T(4,128)}) custom-call(bf16[384,1024]{1,0:T(8,128)(2,1)} %get-tuple-element.15.in_grad, bf16[256,1408]{1,0:T(8,128)(2,1)} %get-tuple-element.16.gate, bf16[256,1408]{1,0:T(8,128)(2,1)} %get-tuple-element.17.value, ...), custom_call_target="tpu_custom_call" | custom-call | tf_op jit(solution)/shard_map/store_all/pallas_call | solution.py:1369
where the time goes:
time: 117 us; the launch traced here: 116 us
  Pallas kernels  116 us (99%)
    pallas_call x1, Pallas kernels, fused_all(): pl.pallas_call(functools.partial(fused_kernel, (deep, across, width), fac...  113 us
    pallas_call x1, Pallas kernels, store_all(): pl.pallas_call(store_kernel, out_shape=tuple(outs), in_specs=[hbm] * 5, o...  3.13 us

commit v1 on v0

--- a/solution.py
+++ b/solution.py
@@ -512,18 +512,18 @@
 
 TUNED = (
     ("weights_y", 0), ("weights_y", 1), ("tokens_x", 0), ("own", 2), ("own", 0), ("tokens_y", 1), ("near", 0),
-    ("tokens_x", 2), ("relay", 0, 1, False), ("relay", 0, 1, True), ("tokens_x", 1), ("relay", 0, 2, False),
-    ("tokens_y", 0), ("near", 1), ("weights_y", 2), ("edge_out", 0), ("edge_out", 1), ("take", 1, 0, 2),
-    ("take", 0, 1, 1), ("relay", 0, 2, True), ("relay", 2, 1, False), ("own", 1), ("take", 0, 1, 0),
-    ("relay", 1, 1, True), ("relay", 1, 1, False), ("edge_share", 0), ("edge_share", 1), ("tokens_y", 2), ("near", 2),
-    ("take", 1, 1, 1), ("last", 0), ("take", 1, 0, 0), ("relay", 1, 2, False), ("cots", 0), ("take", 1, 0, 1),
-    ("tokens_core",), ("edge_pass", 0), ("edge_pass", 1), ("take", 1, 1, 2), ("take", 1, 1, 0), ("take", 0, 1, 2),
-    ("take_rest",), ("project", 0), ("mix", 0), ("relay", 1, 2, True), ("relay", 2, 1, True), ("cots", 1),
-    ("weight", 0), ("last", 1), ("relay", 2, 2, False), ("project", 1), ("relay", 2, 2, True), ("pass_on", 0, 2),
-    ("cots", 2), ("mix", 1), ("weight", 1), ("pass_on", 0, 1), ("last", 2), ("project", 2), ("mix", 2), ("input", 0),
-    ("finish", 0), ("first", 0), ("input", 2), ("pass_on", 1, 2), ("weight", 2), ("owners", 0), ("first", 2),
-    ("input", 1), ("taps",), ("pass_on", 1, 1), ("first", 1), ("second", 1), ("pass_on", 2, 2), ("finish", 1),
-    ("second", 0), ("pass_on", 2, 1), ("owners", 1), ("input", 3), ("finish", 2), ("taps_sum",), ("owners", 2),
+    ("tokens_x", 2), ("relay", 0, 1, False), ("relay", 0, 1, True), ("tokens_y", 0), ("tokens_x", 1), ("near", 1),
+    ("weights_y", 2), ("edge_out", 0), ("relay", 0, 2, False), ("edge_out", 1), ("take", 1, 0, 2), ("take", 0, 1, 1),
+    ("relay", 0, 2, True), ("relay", 2, 1, False), ("own", 1), ("take", 0, 1, 0), ("edge_share", 0),
+    ("edge_share", 1), ("tokens_y", 2), ("relay", 1, 1, False), ("take", 1, 1, 1), ("relay", 1, 1, True), ("near", 2),
+    ("last", 0), ("take", 1, 0, 0), ("relay", 1, 2, False), ("cots", 0), ("take", 1, 0, 1), ("edge_pass", 0),
+    ("edge_pass", 1), ("tokens_core",), ("take", 1, 1, 2), ("take", 1, 1, 0), ("take", 0, 1, 2), ("take_rest",),
+    ("project", 0), ("mix", 0), ("relay", 1, 2, True), ("relay", 2, 1, True), ("cots", 1), ("weight", 0), ("last", 1),
+    ("relay", 2, 2, False), ("project", 1), ("pass_on", 0, 2), ("relay", 2, 2, True), ("cots", 2), ("mix", 1),
+    ("weight", 1), ("pass_on", 0, 1), ("last", 2), ("project", 2), ("mix", 2), ("input", 0), ("finish", 0),
+    ("first", 0), ("input", 2), ("pass_on", 1, 2), ("weight", 2), ("owners", 0), ("first", 2), ("input", 1),
+    ("taps",), ("pass_on", 1, 1), ("first", 1), ("second", 1), ("pass_on", 2, 2), ("finish", 1), ("second", 0),
+    ("pass_on", 2, 1), ("owners", 1), ("input", 3), ("finish", 2), ("taps_sum",), ("owners", 2),
 )
 
 
@@ -641,8 +641,8 @@
     blocks = feats // rows
     first_feats = feats * 3 // 8 // LANES * LANES
     spans = ((0, first_feats), (first_feats, feats - first_feats))
-    step = tokens * 3 // 8 // 16 * 16
-    pieces = ((0, step), (step, step), (2 * step, tokens - 2 * step))
+    cuts = [tokens * k // 16 // 16 * 16 for k in (0, 6, 12, 16)]
+    pieces = tuple((low, high - low) for low, high in zip(cuts, cuts[1:]))
     last = len(pieces) - 1
     weights = (gate_w, value_w)
     outs = (gate_out, value_out)
@@ -956,7 +956,7 @@
 
     def weight_terms(c):
         def visit(level):
-            for yy in range(across):
+            for yy in (ny, y):
                 block = level * across + yy
                 at = pl.ds(pl.multiple_of(block * rows, rows), rows)
                 total = sum(
@@ -969,7 +969,7 @@
             for up in (True, False):
                 @pl.when((level > z) & (z == 0) if up else (level < z) & (z == deep - 1))
                 def _():
-                    for yy in range(across):
+                    for yy in (ny, y):
                         sum_hop(c, level * across + yy, up, start)
 
         far_first(visit)
@@ -981,7 +981,7 @@
             @pl.when((z > 0) & (z < deep - 1) & ((level < deep) if up else (level >= 0)))
             def _():
                 way = 0 if up else 1
-                for yy in range(across):
+                for yy in (ny, y):
                     block = level * across + yy
                     landed(from_z.at[way, c, block], sz_recv.at[way, c, block])
                     total = grads[c, block].astype(jnp.float32) + from_z[way, c, block].astype(jnp.float32)
@@ -1052,19 +1052,20 @@
         r, yy = moved(rep, dr), moved(y, dy)
         q = part_of(r, yy)
 
-        @pl.loop(0, 2 * blocks)
-        def _(i):
-            half = jnp.where(i < blocks, ntp, tp)
-            j = i % blocks
-            total = sum(
-                lax.dot_general(
-                    cot[r, token_rows(yy), chunk_lanes(c)], w_all[c, half * blocks + j],
-                    (((1,), (1,)), ((), ())), preferred_element_type=jnp.float32,
-                ) for c in range(chunks)
-            )
-            pv[half, q, :, pl.ds(pl.multiple_of(j * rows, rows), rows)] = total.astype(pv.dtype)
-
+        def terms_of(half):
+            @pl.loop(0, blocks)
+            def _(j):
+                total = sum(
+                    lax.dot_general(
+                        cot[r, token_rows(yy), chunk_lanes(c)], w_all[c, half * blocks + j],
+                        (((1,), (1,)), ((), ())), preferred_element_type=jnp.float32,
+                    ) for c in range(chunks)
+                )
+                pv[half, q, :, pl.ds(pl.multiple_of(j * rows, rows), rows)] = total.astype(pv.dtype)
+
+        terms_of(ntp)
         tp_hop(q, start)
+        terms_of(tp)
 
     def tp_hop(q, sink):
         sink(remote(pv.at[ntp, q], from_tp.at[q], tp_send.at[q], tp_recv.at[q], tp=ntp))
@@ -1340,24 +1341,28 @@
 
 def store_kernel(in_grad, gate, value, gate_taps, value_taps, *refs):
     outs, held, (gate_wide, value_wide, load_sem, sem) = refs[:5], refs[5:10], refs[10:]
-    loads = [
-        pltpu.make_async_copy(src, dst, load_sem.at[k])
-        for k, (src, dst) in enumerate(zip((in_grad, gate, value, gate_taps, value_taps), held))
-    ]
-    order = (1, 2, 0, 3, 4)
-    for k in order:
-        loads[k].start()
-    copies = []
-    for k in order:
-        loads[k].wait()
-        src = held[k]
+    sources = (in_grad, gate, value, gate_taps, value_taps)
+    count = load_sem.shape[1]
+
+    def split(k):
+        rows = sources[k].shape[0]
+        size = rows // count
+        return [pl.ds(p * size, size) for p in range(count)] if size % 16 == 0 and size * count == rows else [pl.ds(0, rows)]
+
+    tasks = [(k, p, at) for k in (1, 2, 0, 3, 4) for p, at in enumerate(split(k))]
+    loads = [pltpu.make_async_copy(sources[k].at[at], held[k].at[at], load_sem.at[k, p]) for k, p, at in tasks]
+    for load in loads:
+        load.start()
+    stores = []
+    for (k, p, at), load in zip(tasks, loads):
+        load.wait()
+        src = {1: gate_wide, 2: value_wide}.get(k, held[k])
         if k in (1, 2):
-            src = gate_wide if k == 1 else value_wide
-            src[...] = held[k][...].astype(src.dtype)
-        copies.append(pltpu.make_async_copy(src, outs[k], sem.at[k]))
-        copies[-1].start()
-    for copy in copies:
-        copy.wait()
+            src[at] = held[k][at].astype(src.dtype)
+        stores.append(pltpu.make_async_copy(src.at[at], outs[k].at[at], sem.at[k, p]))
+        stores[-1].start()
+    for store in stores:
+        store.wait()
 
 
 def store_all(*arrays):
@@ -1365,7 +1370,7 @@
     wide = jax.ShapeDtypeStruct(arrays[1].shape, jnp.float32)
     outs = [jax.ShapeDtypeStruct(a.shape, a.dtype) for a in arrays]
     outs[1:3] = wide, wide
-    sem = pltpu.SemaphoreType.DMA((5,))
+    sem = pltpu.SemaphoreType.DMA((5, 4))
     return pl.pallas_call(
         store_kernel,
         out_shape=tuple(outs),

time: 117 us -> 117 us (level); the launches traced: 116 us -> 115 us
    pallas_call x1, Pallas kernels: 113 us -> 111 us  [fused_all(): pl.pallas_call(functools.partial(fused_kernel, (deep, across, width), fac...]
where the time goes in v1:
time: 117 us; the launch traced here: 115 us
  Pallas kernels  115 us (98%)
    pallas_call x1, Pallas kernels, fused_all(): pl.pallas_call(functools.partial(fused_kernel, (deep, across, width), fac...  111 us
    pallas_call x1, Pallas kernels, store_all(): pl.pallas_call(store_kernel, out_shape=tuple(outs), in_specs=[hbm] * 5, o...  3.14 us

profile of v1, /device:TPU:0, one launch (start us, length us, event | category | flops | bytes accessed | tf_op | source)
XLA Modules:
  0.0 115.3 jit_solution(5580160091631291120)
XLA Ops:
  0.6 111.5 %fused_all.1 = (bf16[384,1024]{1,0:T(8,128)(2,1)}, bf16[256,1408]{1,0:T(8,128)(2,1)}, bf16[256,1408]{1,0:T(8,128)(2,1)}, f32[3,2816]{1,0:T(4,128)}, f32[3,2816]{1,0:T(4,128)}) custom-call(bf16[384,1024]{1,0:T(8,128)(2,1)} %bitcast.4, bf16[256,1408]{1,0:T(8,128)(2,1)} %gate_w.1, bf16[256,1408]{1,0:T(8,128)(2,1)} %value_w.1, f32[3,2816]{1,0:T(4,128)} %gate_taps.1, ...), custom_call_target="tpu_custom_call" | custom-call | tf_op jit(solution)/shard_map/fused_all/pallas_call | solution.py:1325
  112.1 3.1 %store_all.1 = (bf16[384,1024]{1,0:T(8,128)(2,1)}, f32[256,1408]{1,0:T(8,128)}, f32[256,1408]{1,0:T(8,128)}, f32[3,2816]{1,0:T(4,128)}, f32[3,2816]{1,0:T(4,128)}) custom-call(bf16[384,1024]{1,0:T(8,128)(2,1)} %get-tuple-element.15.in_grad, bf16[256,1408]{1,0:T(8,128)(2,1)} %get-tuple-element.16.gate, bf16[256,1408]{1,0:T(8,128)(2,1)} %get-tuple-element.17.value, ...), custom_call_target="tpu_custom_call" | custom-call | tf_op jit(solution)/shard_map/store_all/pallas_call | solution.py:1374

commit v2 on v1

--- a/solution.py
+++ b/solution.py
@@ -1249,10 +1249,6 @@
     )
     for name, *args in plan(chunks, deep):
         actions[name](*args)
-    input_last()
-    taps_last()
-    for c in range(chunks):
-        owners_last(c)
     for side in range(2):
         edge_out(side, sent)
         edge_share(side, sent)
@@ -1272,6 +1268,11 @@
             for near_block in (False, True):
                 w_relay(c, dist, near_block, sent)
         g_direct(c, sent)
+    input_last()
+    taps_last()
+    for c in range(chunks):
+        owners_last(c)
+    for c in range(chunks):
         sums_sent(c)
 
         @pl.when(live(part, c))

time: 117 us -> 116 us (level)
  no operation moved by 1% of the time
where the time goes in v2:
time: 116 us; the launch traced here: 115 us
  Pallas kernels  115 us (99%)
    pallas_call x1, Pallas kernels, fused_all(): pl.pallas_call(functools.partial(fused_kernel, (deep, across, width), fac...  111 us
    pallas_call x1, Pallas kernels, store_all(): pl.pallas_call(store_kernel, out_shape=tuple(outs), in_specs=[hbm] * 5, o...  3.14 us

profile of v2, /device:TPU:0, one launch (start us, length us, event | category | flops | bytes accessed | tf_op | source)
XLA Modules:
  0.0 115.2 jit_solution(2733465508492584671)
XLA Ops:
  0.6 111.4 %fused_all.1 = (bf16[384,1024]{1,0:T(8,128)(2,1)}, bf16[256,1408]{1,0:T(8,128)(2,1)}, bf16[256,1408]{1,0:T(8,128)(2,1)}, f32[3,2816]{1,0:T(4,128)}, f32[3,2816]{1,0:T(4,128)}) custom-call(bf16[384,1024]{1,0:T(8,128)(2,1)} %bitcast.4, bf16[256,1408]{1,0:T(8,128)(2,1)} %gate_w.1, bf16[256,1408]{1,0:T(8,128)(2,1)} %value_w.1, f32[3,2816]{1,0:T(4,128)} %gate_taps.1, ...), custom_call_target="tpu_custom_call" | custom-call | tf_op jit(solution)/shard_map/fused_all/pallas_call | solution.py:1326
  112.1 3.1 %store_all.1 = (bf16[384,1024]{1,0:T(8,128)(2,1)}, f32[256,1408]{1,0:T(8,128)}, f32[256,1408]{1,0:T(8,128)}, f32[3,2816]{1,0:T(4,128)}, f32[3,2816]{1,0:T(4,128)}) custom-call(bf16[384,1024]{1,0:T(8,128)(2,1)} %get-tuple-element.15.in_grad, bf16[256,1408]{1,0:T(8,128)(2,1)} %get-tuple-element.16.gate, bf16[256,1408]{1,0:T(8,128)(2,1)} %get-tuple-element.17.value, ...), custom_call_target="tpu_custom_call" | custom-call | tf_op jit(solution)/shard_map/store_all/pallas_call | solution.py:1375
